TPU v7x, 32 devices: a whole 2x2x4 slice. The times are simulated.
32 devices in a mesh: ep: 4 (over y, x), tp: 8 (over z, core).
Axes of the slice: x: 2, y: 2, z: 4, core: 2. Of those that a mesh axis runs over, the one named last changes fastest.
Arguments:
- tokens: bfloat16 [4096, 2048], P('ep', 'tp'), may hold values from -48 to 48
- pre_gain: bfloat16 [2048], P('tp'), may hold values from 0.099609375 to 1.8984375
- route_ids: int32 [4096, 2], P('ep'), may hold values from 0 to 3, all different within a row; in each aligned block of 1024 rows (0 to 1023, 1024 to 2047, ...) at most 576 rows name the same one
- route_weights: float32 [4096, 2], P('ep'), may hold values from 0.1 to 1
- gate_weight: bfloat16 [4, 2048, 7168], P('ep', None, 'tp'), may hold values from -0.125 to 0.125
- up_weight: bfloat16 [4, 2048, 7168], P('ep', None, 'tp'), may hold values from -0.125 to 0.125
- down_weight: bfloat16 [4, 7168, 2048], P('ep', 'tp')
- post_gain: bfloat16 [2048], P('tp'), may hold values from 0.099609375 to 1.8984375
Outputs:
- mixed: bfloat16 [4096, 2048], P('ep', 'tp')
Inputs may be any that keep to these rules, and one draw needn't show every extreme that they name: `route_ids`: each row names 2 different experts; among the rows of one index of ep no expert is named more than 576 times, a bound that some block reaches.
All inputs are finite; a program needn't handle non-finite values.
Results may differ from a plain program's by a relative error of at most 0.02.
Values may be sent and summed in bfloat16 or wider, within the bound.
A program may use at most 128 MiB of HBM per device.

v0:
```python
import jax
import jax.numpy as jnp
from jax import lax
from jax.sharding import PartitionSpec as P

D = 2048


epsilon = 1e-06


def run_expert(routed, gate_weight, up_weight, down_weight):
    gate_block = gate_weight[0]
    up_block = up_weight[0]
    down_block = down_weight[0]
    piece = lax.all_gather(routed, "tp", axis=1, tiled=True)
    gate_act = jnp.dot(piece, gate_block, preferred_element_type=jnp.float32)
    up_act = jnp.dot(piece, up_block, preferred_element_type=jnp.float32)
    hidden = (jax.nn.silu(gate_act) * up_act).astype(jnp.bfloat16)
    partial_value = jnp.dot(hidden, down_block, preferred_element_type=jnp.float32)
    return lax.psum_scatter(
        partial_value.astype(jnp.bfloat16), "tp", scatter_dimension=1, tiled=True
    )


def on_device(
    tokens, pre_gain, route_ids, route_weights, gate_weight, up_weight, down_weight, post_gain
):
    tok_rows, columns = tokens.shape
    top_count = route_ids.shape[1]
    groups = lax.axis_size("ep")
    capacity = 9 * tok_rows * top_count // (8 * groups)
    values = tokens.astype(jnp.float32)
    squares = lax.psum(jnp.sum(values * values, axis=1), "tp")
    normed = (
        values * lax.rsqrt(squares / D + epsilon)[:, None] * pre_gain.astype(jnp.float32)[None, :]
    ).astype(jnp.bfloat16)
    flat_ids = route_ids.reshape(-1)
    onehot = (flat_ids[:, None] == jnp.arange(groups, dtype=jnp.int32)[None, :]).astype(jnp.int32)
    slot_rank = jnp.sum((jnp.cumsum(onehot, axis=0) - 1) * onehot, axis=1)
    positions = jnp.arange(tok_rows * top_count, dtype=jnp.int32)
    slot_table = (
        jnp.full((groups, capacity), tok_rows * top_count, jnp.int32)
        .at[flat_ids, slot_rank]
        .set(positions)
    )
    padded = jnp.concatenate([normed, jnp.zeros((1, columns), jnp.bfloat16)], axis=0)
    outgoing = padded[slot_table // top_count]
    arrived = lax.all_to_all(outgoing, "ep", split_axis=0, concat_axis=0, tiled=True)
    results = run_expert(arrived.reshape(-1, columns), gate_weight, up_weight, down_weight)
    returned = lax.all_to_all(
        results.reshape(groups, capacity, columns), "ep", split_axis=0, concat_axis=0, tiled=True
    )
    copies = returned.reshape(-1, columns)[flat_ids * capacity + slot_rank]
    copies = copies.astype(jnp.float32).reshape(tok_rows, top_count, columns)
    combined = jnp.sum(copies * route_weights[:, :, None], axis=1)
    totals = lax.psum(jnp.sum(combined * combined, axis=1), "tp")
    scaled = combined * lax.rsqrt(totals / D + epsilon)[:, None]
    return (scaled * post_gain.astype(jnp.float32)[None, :]).astype(jnp.bfloat16)


def solution(mesh):
    placed = (
        P("ep", "tp"),
        P("tp"),
        P("ep", None),
        P("ep", None),
        P("ep", None, "tp"),
        P("ep", None, "tp"),
        P("ep", "tp", None),
        P("tp"),
    )
    return jax.shard_map(
        on_device, mesh=mesh, in_specs=placed, out_specs=P("ep", "tp"), check_vma=False
    )
```

profile of v0, /device:TPU:0, one launch (start us, length us, event | category | flops | bytes accessed | tf_op | source)
XLA Modules:
  0.0 351.4 jit_solution(1468123328249133810)
XLA Ops:
  6.5 0.9 copy.10
  8.0 0.3 reshape.107
  8.3 1.2 reduce-window.6
  10.1 0.7 multiply_reduce_fusion.2
  10.8 0.8 and_reduce_fusion
  11.6 8.1 %scatter_custom_fusion = s32[2304]{0:T(1024)S(1)} fusion(s32[2048]{0:T(1024)S(1)} %broadcast_select_fusion, s32[2048]{0:T(1024)S(1)} %iota.11, s32[]{:T(128)} %constant.37.clone.1), kind=kCustom, calls=%fused_computation.41 | custom fusion | bytes 9220
  19.9 1.3 fusion.6
  21.1 18.1 %psum.14 = f32[1024]{0:T(1024)S(1)} all-reduce(f32[1024]{0:T(1024)S(1)} %fusion.6), channel_id=1, replica_groups=mesh['ep'=4,'tp'=8] {'tp'}, use_global_device_ids=true, to_apply=%region_1.0 | all-reduce | flops 1024 | bytes 8192 | tf_op jit(solution)/shard_map/psum | solution.py:34
  39.2 0.7 convert_element_type.34
  39.9 1.2 fusion.8
  41.2 6.9 %gather_fusion = bf16[2304,256]{1,0:T(8,128)(2,1)S(1)} fusion(bf16[1025,256]{1,0:T(8,128)(2,1)S(1)} %concatenate.6, s32[3072]{0:T(1024)S(1)} %pad_clamp_fusion), kind=kCustom, calls=%fused_computation | custom fusion | bytes 2368512 | tf_op jit(solution)/shard_map/gather | solution.py:48
  48.1 16.3 %all_to_all.10 = bf16[4,576,256]{2,1,0:T(8,128)(2,1)} all-to-all(bf16[4,576,256]{2,1,0:T(8,128)(2,1)S(1)} %bitcast.34), channel_id=1, replica_groups=mesh['ep'=4,'tp'=8] {'ep'}, dimensions={0} | all-to-all | bytes 2359296 | tf_op jit(solution)/shard_map/all_to_all | solution.py:49
  64.5 89.0 %all-gather.2.cloned.1.call-done = bf16[2304,2048]{1,0:T(8,128)(2,1)} async-done(((bf16[2304,256]{1,0:T(8,128)(2,1)}), bf16[2304,2048]{1,0:T(8,128)(2,1)}) %all-gather.2.cloned.1.call-update) | async-done | bytes 9437200 | tf_op jit(solution)/shard_map/all_gather | solution.py:16
  153.5 15.6 %fusion.4 = f32[2304,896]{1,0:T(8,128)} fusion(bf16[2304,2048]{1,0:T(8,128)(2,1)} %all-gather.2.cloned.1.call-done, bf16[1,2048,896]{2,1,0:T(8,128)(2,1)} %param.12), kind=kOutput, calls=%fused_computation.8 | convolution fusion | flops 8455716864 | bytes 21364736 | tf_op jit(solution)/shard_map/dot_general | solution.py:17
  169.1 26.9 %convolution_convert_fusion = bf16[2304,2048]{1,0:T(8,128)(2,1)} fusion(f32[2304,896]{1,0:T(8,128)} %fusion.4, bf16[2304,2048]{1,0:T(8,128)(2,1)} %all-gather.2.cloned.1.call-done, bf16[1,896,2048]{2,1,0:T(8,128)(2,1)} %param.14, bf16[1,2048,896]{2,1,0:T(8,128)(2,1)} %param.13), kind=kOutput, calls=%fused_computation.3 | convolution fusion | flops 16928538624 | bytes 34471936 | tf_op jit(solution)/shard_map/dot_general | solution.py:20
  196.0 97.8 %reduce-scatter.2.cloned.1.call-done = bf16[2304,256]{1,0:T(8,128)(2,1)} async-done(((bf16[2304,2048]{1,0:T(8,128)(2,1)}), bf16[2304,256]{1,0:T(8,128)(2,1)}) %reduce-scatter.2.cloned.1.call-update) | async-done | bytes 1179664 | tf_op jit(solution)/shard_map/reduce_scatter | solution.py:21
  293.8 3.7 %all-to-all-start.1 = ((bf16[4,576,256]{2,1,0:T(8,128)(2,1)}), bf16[4,576,256]{2,1,0:T(8,128)(2,1)S(1)}, u32[]{:S(2)}, u32[]{:S(2)}) async-start(bf16[4,576,256]{2,1,0:T(8,128)(2,1)} %bitcast.36), calls=%async_computation.2 | async-start | bytes 2359296 | tf_op jit(solution)/shard_map/all_to_all | solution.py:51
  297.5 1.0 copy.13
  298.6 12.2 %all-to-all-done.1 = bf16[4,576,256]{2,1,0:T(8,128)(2,1)S(1)} async-done(((bf16[4,576,256]{2,1,0:T(8,128)(2,1)}), bf16[4,576,256]{2,1,0:T(8,128)(2,1)S(1)}, u32[]{:S(2)}, u32[]{:S(2)}) %all-to-all-start.1) | async-done | bytes 1179680 | tf_op jit(solution)/shard_map/all_to_all | solution.py:51
  310.7 9.0 %gather_fusion.1 = bf16[2048,256]{1,0:T(8,128)(2,1)} fusion(bf16[2304,256]{1,0:T(8,128)(2,1)S(1)} %bitcast.33, s32[2048]{0:T(1024)S(1)} %broadcast_clamp_fusion), kind=kCustom, calls=%fused_computation.1 | custom fusion | bytes 2105344 | tf_op jit(solution)/shard_map/gather | solution.py:54
  319.7 2.1 reshape.116
  321.8 6.5 %multiply_reduce_fusion = f32[1024,256]{1,0:T(8,128)S(1)} fusion(f32[1024,2,256]{2,1,0:T(2,128)S(1)} %reshape.116, f32[1024,2]{1,0:T(8,128)} %copy.13), kind=kLoop, calls=%fused_computation.10 | loop fusion | flops 786432 | bytes 3153920 | tf_op jit(solution)/shard_map/reduce_sum | solution.py:56
  328.6 14.9 %psum.15 = f32[1024]{0:T(1024)S(1)} all-reduce(f32[1024]{0:T(1024)S(1)} %multiply_reduce_fusion.1), channel_id=1, replica_groups=mesh['ep'=4,'tp'=8] {'tp'}, use_global_device_ids=true, to_apply=%region_9.10 | all-reduce | flops 1024 | bytes 8192 | tf_op jit(solution)/shard_map/psum | solution.py:57
  343.5 1.0 multiply_convert_fusion.1
  (28 shorter events, 1.7 us)
Async XLA Ops:
  6.5 147.0 %all-gather.2.cloned.1.call-start = ((), (), s32[]{:S(2)}) async-start(), calls=%async_computation.3 | async-start | bytes 10616832 | tf_op jit(solution)/shard_map/all_gather | solution.py:16
  64.4 229.4 %reduce-scatter.2.cloned.1.call-start = ((), (), s32[]{:S(2)}) async-start(), calls=%async_computation.4 | async-start | bytes 10616832 | tf_op jit(solution)/shard_map/reduce_scatter | solution.py:21
  196.0 101.5 %copy-start = (f32[1024,2]{0,1:T(2,128)S(1)}, f32[1024,2]{0,1:T(2,128)}, u32[]{:S(2)}) copy-start(f32[1024,2]{0,1:T(2,128)} %param.11) | copy-start | bytes 24580
  196.0 102.6 %copy-start.1 = (bf16[256]{0:T(256)(128)(2,1)S(1)}, bf16[256]{0:T(256)(128)(2,1)}, u32[]{:S(2)}) copy-start(bf16[256]{0:T(256)(128)(2,1)} %param.15) | copy-start | bytes 1540
  293.8 17.0 %all-to-all-start.1 = ((bf16[4,576,256]{2,1,0:T(8,128)(2,1)}), bf16[4,576,256]{2,1,0:T(8,128)(2,1)S(1)}, u32[]{:S(2)}, u32[]{:S(2)}) async-start(bf16[4,576,256]{2,1,0:T(8,128)(2,1)} %bitcast.36), calls=%async_computation.2 | async-start | bytes 2359296 | tf_op jit(solution)/shard_map/all_to_all | solution.py:51
Sparse Core Ops, SparseCore 0:
  64.5 88.9 all-gather.1
  196.1 97.6 reduce-scatter.1
where the time goes:
time: 352 us; the launch traced here: 351 us
  waiting for transfers between devices  199 us (57%)
  blocking collectives  49.4 us (14%)
  matrix products  42.5 us (12%)
  local copies, waits for them, and re-layouts  29.2 us (8%)
  other arithmetic  14 us (4%)
  between operations  13.5 us (4%)
  starting transfers between devices  3.75 us (1%)
    reduce_scatter x1, waiting for transfers between devices, run_expert(): lax.psum_scatter(partial_value.astype(jnp.bfloat16), 'tp', scatter_dimens...  97.8 us
    all_gather x1, waiting for transfers between devices, run_expert(): piece = lax.all_gather(routed, 'tp', axis=1, tiled=True)  89 us
    dot_general x1, matrix products, run_expert(): jnp.dot(hidden, down_block, preferred_element_type=jnp.float32)  26.9 us
    psum x1, blocking collectives, on_device(): squares = lax.psum(jnp.sum(values * values, axis=1), 'tp')  18.1 us
    all_to_all x1, blocking collectives, on_device(): lax.all_to_all(outgoing, 'ep', split_axis=0, concat_axis=0, tiled=True)  16.3 us
    dot_general x1, matrix products, run_expert(): gate_act = jnp.dot(piece, gate_block, preferred_element_type=jnp.float32)  15.6 us
    psum x1, blocking collectives, on_device(): totals = lax.psum(jnp.sum(combined * combined, axis=1), 'tp')  14.9 us
    all_to_all x1, waiting for transfers between devices, on_device(): lax.all_to_all(results.reshape(groups, capacity, columns), 'ep', split_ax...  12.2 us
  transfers between devices with their start and end apart: 3, of which 3 were waited for; matrix products, arithmetic and copies ran while one was open for 0% of the time, Pallas kernels for 0%

commit v1 on v0

v1 whole, which is shorter than its diff:
```python
import functools

import jax
import jax.numpy as jnp
from jax import lax
from jax.experimental import pallas as pl
from jax.experimental.pallas import tpu as pltpu
from jax.sharding import PartitionSpec as P

epsilon = 1e-06
MESH = pl.DeviceIdType.MESH
DMA = pltpu.SemaphoreType.DMA
BF16 = jnp.bfloat16


def greet(targets):
    barrier = pltpu.get_barrier_semaphore()
    for target in targets:
        pl.semaphore_signal(barrier, inc=1, device_id=target, device_id_type=MESH)
    pl.semaphore_wait(barrier, len(targets))


def exchange_kernel(n, x_ref, out_ref, buf, send, recv):
    me = lax.axis_index("tp")
    peers = [{"tp": lax.rem(me + k, n)} for k in range(1, n)]
    greet(peers)
    copies = []
    for k in range(1, n):
        copy = pltpu.make_async_remote_copy(
            src_ref=x_ref, dst_ref=buf.at[k - 1], send_sem=send.at[k - 1],
            recv_sem=recv.at[k - 1], device_id=peers[k - 1], device_id_type=MESH,
        )
        copy.start()
        copies.append(copy)
    total = x_ref[...]
    for k in range(1, n):
        copies[k - 1].wait_recv()
        total = total + buf[k - 1]
    out_ref[...] = total
    for copy in copies:
        copy.wait_send()


def sum_over_tp(rows, number):
    n = lax.axis_size("tp")
    x = rows.reshape(-1, 128)
    total = pl.pallas_call(
        functools.partial(exchange_kernel, n),
        out_shape=jax.ShapeDtypeStruct(x.shape, jnp.float32),
        in_specs=[pl.BlockSpec(memory_space=pltpu.VMEM)],
        out_specs=pl.BlockSpec(memory_space=pltpu.VMEM),
        scratch_shapes=[pltpu.VMEM((n - 1,) + x.shape, jnp.float32), DMA((n - 1,)), DMA((n - 1,))],
        compiler_params=pltpu.CompilerParams(collective_id=number, has_side_effects=True),
        name="exchange%d" % number,
    )(x)
    return total.reshape(-1)


def places(groups, layers):
    me, g = lax.axis_index("tp"), lax.axis_index("ep")
    core, z = lax.rem(me, 2), me // 2
    return core, z, g, {"tp": me + 1 - 2 * core}


def greet_all(groups, layers, core, z, g, partner):
    targets = [partner]
    targets += [{"tp": lax.rem(z + k, layers) * 2 + core} for k in range(1, layers)]
    targets += [{"ep": lax.rem(g + m, groups)} for m in range(1, groups)]
    greet(targets)


def dispatch_kernel(
    groups, layers, cap, cols, x_ref, s_ref, out_ref, zbuf, obuf, zs, zr, es, er, ds, dr, ls
):
    core, z, g, partner = places(groups, layers)
    greet_all(groups, layers, core, z, g, partner)

    def z_copy(k):
        return pltpu.make_async_remote_copy(
            src_ref=x_ref, dst_ref=zbuf.at[k], send_sem=zs.at[k], recv_sem=zr.at[k],
            device_id={"tp": lax.rem(z + k, layers) * 2 + core}, device_id_type=MESH,
        )

    def area(k, m, of):
        source = lax.rem(g + groups - m, groups)
        column = (lax.rem(z + layers - k, layers) * 2 + of) * cols
        return out_ref.at[
            pl.ds(pl.multiple_of(source * cap, 16), cap), pl.ds(pl.multiple_of(column, 128), cols)
        ]

    def e_copy(k, m):
        return pltpu.make_async_remote_copy(
            src_ref=obuf.at[k, m], dst_ref=area(k, 0, core), send_sem=es.at[k, m],
            recv_sem=er.at[k, m], device_id={"ep": lax.rem(g + m, groups)}, device_id_type=MESH,
        )

    def d_copy(k, m, source):
        return pltpu.make_async_remote_copy(
            src_ref=source, dst_ref=area(k, m, core), send_sem=ds.at[k, m],
            recv_sem=dr.at[k, m], device_id=partner, device_id_type=MESH,
        )

    def l_copy(k):
        return pltpu.make_async_copy(obuf.at[k, 0], area(k, 0, core), ls.at[k])

    for k in range(1, layers):
        z_copy(k).start()
    zbuf[0] = x_ref[...]

    def forward(k):
        @pl.loop(1, groups)
        def _(m):
            e_copy(k, m).wait_recv()
            d_copy(k, m, area(k, m, core)).start()

    @pl.loop(0, layers)
    def _(k):
        @pl.when(k > 0)
        def _():
            z_copy(k).wait_recv()

        @pl.loop(0, groups)
        def _(i):
            m = lax.rem(i + 1, groups)
            obuf[k, m] = jnp.dot(
                s_ref[lax.rem(g + m, groups)], zbuf[k], preferred_element_type=jnp.float32
            ).astype(BF16)

            @pl.when(m > 0)
            def _():
                e_copy(k, m).start()

        l_copy(k).start()
        d_copy(k, 0, obuf.at[k, 0]).start()

        @pl.when(k > 0)
        def _():
            forward(k - 1)

    forward(layers - 1)

    @pl.loop(0, layers)
    def _(k):
        @pl.when(k > 0)
        def _():
            z_copy(k).wait_send()

        l_copy(k).wait()

        @pl.loop(0, groups)
        def _(m):
            @pl.when(m > 0)
            def _():
                e_copy(k, m).wait_send()

            copy = d_copy(k, m, obuf.at[k, 0])
            copy.wait_send()
            copy.wait_recv()


def dispatch(normed, table):
    groups, cap, tok_rows = table.shape
    layers = lax.axis_size("tp") // 2
    cols = normed.shape[1]
    vmem = pl.BlockSpec(memory_space=pltpu.VMEM)
    return pl.pallas_call(
        functools.partial(dispatch_kernel, groups, layers, cap, cols),
        out_shape=jax.ShapeDtypeStruct((groups * cap, 2 * layers * cols), BF16),
        in_specs=[vmem, vmem],
        out_specs=pl.BlockSpec(memory_space=pl.ANY),
        scratch_shapes=[
            pltpu.VMEM((layers, tok_rows, cols), BF16),
            pltpu.VMEM((layers, groups, cap, cols), BF16),
            DMA((layers,)), DMA((layers,)),
            DMA((layers, groups)), DMA((layers, groups)),
            DMA((layers, groups)), DMA((layers, groups)),
            DMA((layers,)),
        ],
        compiler_params=pltpu.CompilerParams(
            collective_id=1, has_side_effects=True, vmem_limit_bytes=56 * 2**20
        ),
        name="dispatch",
    )(normed, table)


def return_kernel(
    groups, layers, cap, cols, p_ref, w_ref, out_ref, lbuf, pbuf, qbuf, rbuf, obuf, fbuf,
    ls, ds, dr, es, er, zs, zr,
):
    core, z, g, partner = places(groups, layers)
    greet_all(groups, layers, core, z, g, partner)
    rows = groups * cap

    def columns(k, of):
        column = (lax.rem(z + k, layers) * 2 + of) * cols
        return p_ref.at[:, pl.ds(pl.multiple_of(column, 128), cols)]

    def l_copy(k):
        return pltpu.make_async_copy(columns(k, core), lbuf.at[k], ls.at[k])

    def d_copy(k):
        return pltpu.make_async_remote_copy(
            src_ref=columns(k, 1 - core), dst_ref=pbuf.at[k], send_sem=ds.at[k],
            recv_sem=dr.at[k], device_id=partner, device_id_type=MESH,
        )

    def e_copy(k, m):
        return pltpu.make_async_remote_copy(
            src_ref=qbuf.at[k, m], dst_ref=rbuf.at[k, pl.ds(pl.multiple_of(g * cap, 16), cap)],
            send_sem=es.at[k, m], recv_sem=er.at[k, m],
            device_id={"ep": lax.rem(g + m, groups)}, device_id_type=MESH,
        )

    def z_copy(k):
        return pltpu.make_async_remote_copy(
            src_ref=obuf.at[k], dst_ref=fbuf.at[k], send_sem=zs.at[k], recv_sem=zr.at[k],
            device_id={"tp": lax.rem(z + k, layers) * 2 + core}, device_id_type=MESH,
        )

    @pl.loop(0, layers)
    def _(i):
        k = lax.rem(i + 1, layers)
        d_copy(k).start()
        l_copy(k).start()

    @pl.loop(0, layers)
    def _(i):
        k = lax.rem(i + 1, layers)
        l_copy(k).wait()
        d_copy(k).wait_recv()

        @pl.loop(0, groups)
        def _(j):
            m = lax.rem(j + 1, groups)
            at = pl.ds(pl.multiple_of(lax.rem(g + m, groups) * cap, 16), cap)
            both = lbuf[k, at].astype(jnp.float32) + pbuf[k, at].astype(jnp.float32)

            @pl.when(m > 0)
            def _():
                qbuf[k, m] = both.astype(BF16)
                e_copy(k, m).start()

            @pl.when(m == 0)
            def _():
                rbuf[k, pl.ds(pl.multiple_of(g * cap, 16), cap)] = both.astype(BF16)

    tok_rows = w_ref.shape[0]
    tile = min(256, tok_rows)

    @pl.loop(0, layers)
    def _(i):
        k = lax.rem(i + 1, layers)

        @pl.loop(1, groups)
        def _(m):
            e_copy(k, m).wait_recv()

        @pl.loop(0, tok_rows // tile)
        def _(t):
            at = pl.ds(pl.multiple_of(t * tile, tile), tile)
            value = jnp.dot(w_ref[at], rbuf[k], preferred_element_type=jnp.float32)

            @pl.when(k > 0)
            def _():
                obuf[k, at] = value.astype(BF16)

            @pl.when(k == 0)
            def _():
                out_ref[at] = value

        @pl.when(k > 0)
        def _():
            z_copy(k).start()

    @pl.loop(1, layers)
    def _(k):
        z_copy(k).wait_recv()
        out_ref[...] += fbuf[k].astype(jnp.float32)

    @pl.loop(0, layers)
    def _(k):
        d_copy(k).wait_send()

        @pl.loop(1, groups)
        def _(m):
            e_copy(k, m).wait_send()

        @pl.when(k > 0)
        def _():
            z_copy(k).wait_send()


def give_back(partials, mixing, groups):
    rows, width = partials.shape
    tok_rows = mixing.shape[0]
    layers = lax.axis_size("tp") // 2
    cols = width // (2 * layers)
    cap = rows // groups
    vmem = pl.BlockSpec(memory_space=pltpu.VMEM)
    return pl.pallas_call(
        functools.partial(return_kernel, groups, layers, cap, cols),
        out_shape=jax.ShapeDtypeStruct((tok_rows, cols), jnp.float32),
        in_specs=[pl.BlockSpec(memory_space=pl.ANY), vmem],
        out_specs=vmem,
        scratch_shapes=[
            pltpu.VMEM((layers, rows, cols), BF16),
            pltpu.VMEM((layers, rows, cols), BF16),
            pltpu.VMEM((layers, groups, cap, cols), BF16),
            pltpu.VMEM((layers, rows, cols), BF16),
            pltpu.VMEM((layers, tok_rows, cols), BF16),
            pltpu.VMEM((layers, tok_rows, cols), BF16),
            DMA((layers,)), DMA((layers,)), DMA((layers,)),
            DMA((layers, groups)), DMA((layers, groups)),
            DMA((layers,)), DMA((layers,)),
        ],
        compiler_params=pltpu.CompilerParams(
            collective_id=2, has_side_effects=True, vmem_limit_bytes=56 * 2**20
        ),
        name="give_back",
    )(partials, mixing)


def on_device(
    tokens, pre_gain, route_ids, route_weights, gate_weight, up_weight, down_weight, post_gain
):
    tok_rows, cols = tokens.shape
    top_count = route_ids.shape[1]
    groups = lax.axis_size("ep")
    width = cols * lax.axis_size("tp")
    cap = 9 * tok_rows * top_count // (8 * groups)
    values = tokens.astype(jnp.float32)
    squares = sum_over_tp(jnp.sum(values * values, axis=1), 0)
    normed = (
        values * lax.rsqrt(squares / width + epsilon)[:, None] * pre_gain.astype(jnp.float32)[None, :]
    ).astype(BF16)

    experts = jnp.arange(groups, dtype=jnp.int32)
    named = route_ids[:, :, None] == experts[None, None, :]
    member = jnp.any(named, axis=1)
    weight = jnp.sum(jnp.where(named, route_weights[:, :, None], 0.0), axis=1)
    spot = jnp.arange(tok_rows, dtype=jnp.int32)
    before = (spot[:, None] > spot[None, :]).astype(BF16)
    rank = jnp.dot(before, member.astype(BF16), preferred_element_type=jnp.float32)
    key = jnp.where(member, rank.astype(jnp.int32), -1)
    slots = jnp.arange(cap, dtype=jnp.int32)
    table = (key.T[:, None, :] == slots[None, :, None]).astype(BF16)
    mixing = jnp.where(key[:, :, None] == slots[None, None, :], weight[:, :, None], 0.0)
    mixing = mixing.astype(BF16).reshape(tok_rows, groups * cap)

    piece = dispatch(normed, table)
    gate_act = jnp.dot(piece, gate_weight[0], preferred_element_type=jnp.float32)
    up_act = jnp.dot(piece, up_weight[0], preferred_element_type=jnp.float32)
    hidden = (jax.nn.silu(gate_act) * up_act).astype(BF16)
    partials = jnp.dot(hidden, down_weight[0], preferred_element_type=jnp.float32).astype(BF16)
    combined = give_back(partials, mixing, groups)
    totals = sum_over_tp(jnp.sum(combined * combined, axis=1), 3)
    scaled = combined * lax.rsqrt(totals / width + epsilon)[:, None]
    return (scaled * post_gain.astype(jnp.float32)[None, :]).astype(BF16)


def solution(mesh):
    placed = (
        P("ep", "tp"),
        P("tp"),
        P("ep", None),
        P("ep", None),
        P("ep", None, "tp"),
        P("ep", None, "tp"),
        P("ep", "tp", None),
        P("tp"),
    )
    return jax.shard_map(
        on_device, mesh=mesh, in_specs=placed, out_specs=P("ep", "tp"), check_vma=False
    )
```

time: 352 us -> 263 us (0.75)
  waiting for transfers between devices: 199 us -> 0 us
  Pallas kernels: 0 us -> 172 us
  blocking collectives: 49.4 us -> 0 us
  between operations: 13.5 us -> 0.06 us
  other arithmetic: 14 us -> 23.8 us
  local copies, waits for them, and re-layouts: 29.2 us -> 24.2 us
  starting transfers between devices: 3.75 us -> 0 us
    pallas_call x0 -> x4, Pallas kernels: none -> 172 us  [the longest x1 85.4 us: give_back(): pl.pallas_call(functools.partial(return_kernel, groups, layers, cap, cols...]
    reduce_scatter x1 -> x0, waiting for transfers between devices: 97.8 us -> none  [run_expert(): lax.psum_scatter(partial_value.astype(jnp.bfloat16), 'tp', scatter_dimens...]
    all_gather x1 -> x0, waiting for transfers between devices: 89 us -> none  [run_expert(): piece = lax.all_gather(routed, 'tp', axis=1, tiled=True)]
    psum x2 -> x0, blocking collectives: 33 us -> none  [the longest x1 18.1 us: on_device(): squares = lax.psum(jnp.sum(values * values, axis=1), 'tp')]
    all_to_all x1 -> x0, blocking collectives: 16.3 us -> none  [on_device(): lax.all_to_all(outgoing, 'ep', split_axis=0, concat_axis=0, tiled=True)]
    gather x2 -> x0, local copies, waits for them, and re-layouts: 15.9 us -> none  [the longest x1 9 us: on_device(): copies = returned.reshape(-1, columns)[flat_ids * capacity + slot_rank]]
    convert_element_type x4 -> x5, other arithmetic: 2.26 us -> 16.8 us  [the longest x1 8.44 us: on_device(): mixing = mixing.astype(BF16).reshape(tok_rows, groups * cap)]
    eq x2 -> x4, local copies, waits for them, and re-layouts: 0.54 us -> 14.7 us  [on_device(): key[:, :, None] == slots[None, None, :]]
  transfers between devices with their start and end apart: 3 -> 0, of which waited for: 3 -> 0; matrix products, arithmetic and copies ran while one was open for 0% -> 0% of each run, Pallas kernels for 0% -> 0%
where the time goes in v1:
time: 263 us; the launch traced here: 262 us
  Pallas kernels  172 us (65%)
  matrix products  41.8 us (16%)
  local copies, waits for them, and re-layouts  24.2 us (9%)
  other arithmetic  23.8 us (9%)
    pallas_call x1, Pallas kernels, give_back(): pl.pallas_call(functools.partial(return_kernel, groups, layers, cap, cols...  85.4 us
    pallas_call x1, Pallas kernels, dispatch(): pl.pallas_call(functools.partial(dispatch_kernel, groups, layers, cap, co...  71.5 us
    dot_general x1, matrix products, on_device(): jnp.dot(hidden, down_weight[0], preferred_element_type=jnp.float32)  26.9 us
    pallas_call x2, Pallas kernels, sum_over_tp(): pl.pallas_call(functools.partial(exchange_kernel, n), out_shape=jax.Shape...  15.5 us
    eq x4, local copies, waits for them, and re-layouts, on_device(): key[:, :, None] == slots[None, None, :]  14.7 us
    dot_general x1, matrix products, on_device(): jnp.dot(piece, gate_weight[0], preferred_element_type=jnp.float32)  14.5 us
    broadcast_in_dim x2, local copies, waits for them, and re-layouts, on_device(): jnp.where(key[:, :, None] == slots[None, None, :], weight[:, :, None], 0.0)  9.49 us
    convert_element_type x1, other arithmetic, on_device(): mixing = mixing.astype(BF16).reshape(tok_rows, groups * cap)  8.44 us

profile of v1, /device:TPU:0, one launch (start us, length us, event | category | flops | bytes accessed | tf_op | source)
XLA Modules:
  0.0 262.3 jit_solution(14006087709242950231)
XLA Ops:
  0.0 0.7 fusion.13
  0.7 0.5 fusion.9
  1.2 4.1 %fusion.s_ref = bf16[4,576,1024]{2,1,0:T(8,128)(2,1)} fusion(s32[4,1024]{1,0:T(4,128)S(1)} %bitcast.24), kind=kLoop, calls=%fused_computation.3 | loop fusion | flops 4718592 | bytes 4734976 | tf_op jit(solution)/shard_map/convert_element_type | solution.py:346
  5.2 1.8 fusion.10
  7.1 8.7 %exchange0.1 = f32[8,128]{1,0:T(8,128)} custom-call(f32[8,128]{1,0:T(8,128)} %bitcast.25), custom_call_target="tpu_custom_call" | custom-call | tf_op jit(solution)/shard_map/exchange0/pallas_call | solution.py:47
  15.8 0.0 copy-start.2
  15.8 0.8 rsqrt_bitcast_fusion.1
  16.6 0.9 convert_element_type.36
  17.5 2.0 fusion.12.x_ref
  19.5 71.5 %dispatch.1 = bf16[2304,2048]{1,0:T(8,128)(2,1)} custom-call(bf16[1024,256]{1,0:T(8,128)(2,1)} %fusion.12.x_ref, bf16[4,576,1024]{2,1,0:T(8,128)(2,1)} %fusion.s_ref), custom_call_target="tpu_custom_call" | custom-call | tf_op jit(solution)/shard_map/dispatch/pallas_call | solution.py:166
  91.0 0.0 copy-done.2
  91.1 14.5 %fusion.6 = f32[2304,896]{1,0:T(8,128)} fusion(bf16[2304,2048]{1,0:T(8,128)(2,1)} %dispatch.1, bf16[1,2048,896]{2,1,0:T(8,128)(2,1)S(1)} %copy-done.2), kind=kOutput, calls=%fused_computation.10 | convolution fusion | flops 8455716864 | bytes 21364736 | tf_op jit(solution)/shard_map/dot_general | solution.py:351
  105.5 26.9 %convolution_convert_fusion.p_ref = bf16[2304,2048]{1,0:T(8,128)(2,1)} fusion(f32[2304,896]{1,0:T(8,128)} %fusion.6, bf16[2304,2048]{1,0:T(8,128)(2,1)} %dispatch.1, bf16[1,896,2048]{2,1,0:T(8,128)(2,1)} %param.14, bf16[1,2048,896]{2,1,0:T(8,128)(2,1)} %param.13), kind=kOutput, calls=%fused_computation | convolution fusion | flops 16928538624 | bytes 34471936 | tf_op jit(solution)/shard_map/dot_general | solution.py:354
  132.4 4.9 %eq.52 = s32[1024,4,576]{0,2,1:T(8,128)} broadcast(s32[1024,4]{0,1:T(4,128)S(1)} %fusion.9), dimensions={0,1} | broadcast | bytes 9453568 | tf_op jit(solution)/shard_map/eq | solution.py:347
  137.4 9.7 %copy.16 = s32[1024,2304]{1,0:T(8,128)} copy(s32[1024,2304]{0,1:T(8,128)} %bitcast.22) | data formatting | bytes 18874368 | tf_op jit(solution)/shard_map/eq | solution.py:347
  147.0 2.8 %broadcast_in_dim.47 = bf16[1024,4,576]{0,2,1:T(8,128)(2,1)} broadcast(bf16[1024,4]{0,1:T(4,128)(2,1)S(1)} %select_reduce_fusion), dimensions={0,1} | broadcast | bytes 4726784 | tf_op jit(solution)/shard_map/jit(_where)/broadcast_in_dim | solution.py:347
  149.8 6.7 %copy.17 = bf16[1024,2304]{1,0:T(8,128)(2,1)} copy(bf16[1024,2304]{0,1:T(8,128)(2,1)} %bitcast.23) | data formatting | bytes 9437184 | tf_op jit(solution)/shard_map/jit(_where)/broadcast_in_dim | solution.py:347
  156.5 0.1 eq.55
  156.6 8.4 %select_convert_fusion.w_ref = bf16[1024,2304]{1,0:T(8,128)(2,1)} fusion(bf16[1024,2304]{1,0:T(8,128)(2,1)} %copy.17, s32[1024,2304]{1,0:T(8,128)} %copy.16, s32[2304]{0:T(1024)S(1)} %eq.55), kind=kLoop, calls=%fused_computation.1 | loop fusion | flops 4718592 | bytes 18883584 | tf_op jit(solution)/shard_map/convert_element_type | solution.py:348
  165.1 85.4 %give_back.1 = f32[1024,256]{1,0:T(8,128)} custom-call(bf16[2304,2048]{1,0:T(8,128)(2,1)} %convolution_convert_fusion.p_ref, bf16[1024,2304]{1,0:T(8,128)(2,1)} %select_convert_fusion.w_ref), custom_call_target="tpu_custom_call" | custom-call | tf_op jit(solution)/shard_map/give_back/pallas_call | solution.py:300
  250.5 2.0 multiply_reduce_fusion
  252.5 6.8 %exchange3.1 = f32[8,128]{1,0:T(8,128)} custom-call(f32[8,128]{1,0:T(8,128)} %bitcast.26), custom_call_target="tpu_custom_call" | custom-call | tf_op jit(solution)/shard_map/exchange3/pallas_call | solution.py:47
  259.3 0.7 rsqrt_bitcast_fusion
  260.0 2.2 multiply_convert_fusion.1
  (9 shorter events, 0.0 us)
Async XLA Ops:
  15.8 75.2 %copy-start.2 = (bf16[1,2048,896]{2,1,0:T(8,128)(2,1)S(1)}, bf16[1,2048,896]{2,1,0:T(8,128)(2,1)}, u32[]{:S(2)}) copy-start(bf16[1,2048,896]{2,1,0:T(8,128)(2,1)} %param.12) | copy-start | bytes 11010052
  137.4 9.7 %copy-start = (s32[1024,2]{0,1:T(2,128)S(1)}, s32[1024,2]{0,1:T(2,128)}, u32[]{:S(2)}) copy-start(s32[1024,2]{0,1:T(2,128)} %param.10) | copy-start | bytes 24580
  137.4 9.7 %copy-start.1 = (f32[1024,2]{0,1:T(2,128)S(1)}, f32[1024,2]{0,1:T(2,128)}, u32[]{:S(2)}) copy-start(f32[1024,2]{0,1:T(2,128)} %param.11) | copy-start | bytes 24580
  165.1 95.0 %copy-start.3 = (bf16[256]{0:T(256)(128)(2,1)S(1)}, bf16[256]{0:T(256)(128)(2,1)}, u32[]{:S(2)}) copy-start(bf16[256]{0:T(256)(128)(2,1)} %param.15) | copy-start | bytes 1540

commit v2 on v1

--- a/solution.py
+++ b/solution.py
@@ -70,9 +70,15 @@
 
 
 def dispatch_kernel(
-    groups, layers, cap, cols, x_ref, s_ref, out_ref, zbuf, obuf, zs, zr, es, er, ds, dr, ls
+    groups, layers, cap, cols, tile, x_ref, key_ref, gate_ref, up_ref, out_ref,
+    zbuf, obuf, sbuf, piece, wbuf, acc, zs, zr, es, er, ds, dr, ws,
 ):
     core, z, g, partner = places(groups, layers)
+    loads = [
+        pltpu.make_async_copy(ref, wbuf.at[i], ws.at[i]) for i, ref in enumerate((gate_ref, up_ref))
+    ]
+    for load in loads:
+        load.start()
     greet_all(groups, layers, core, z, g, partner)
 
     def z_copy(k):
@@ -81,37 +87,64 @@
             device_id={"tp": lax.rem(z + k, layers) * 2 + core}, device_id_type=MESH,
         )
 
-    def area(k, m, of):
+    def area(k, m):
         source = lax.rem(g + groups - m, groups)
-        column = (lax.rem(z + layers - k, layers) * 2 + of) * cols
-        return out_ref.at[
-            pl.ds(pl.multiple_of(source * cap, 16), cap), pl.ds(pl.multiple_of(column, 128), cols)
-        ]
+        return piece.at[core, k, pl.ds(pl.multiple_of(source * cap, 16), cap)]
 
     def e_copy(k, m):
         return pltpu.make_async_remote_copy(
-            src_ref=obuf.at[k, m], dst_ref=area(k, 0, core), send_sem=es.at[k, m],
+            src_ref=obuf.at[k, m], dst_ref=area(k, 0), send_sem=es.at[k, m],
             recv_sem=er.at[k, m], device_id={"ep": lax.rem(g + m, groups)}, device_id_type=MESH,
         )
 
-    def d_copy(k, m, source):
-        return pltpu.make_async_remote_copy(
-            src_ref=source, dst_ref=area(k, m, core), send_sem=ds.at[k, m],
+    def d_copy(k, m):
+        return pltpu.make_async_remote_copy(
+            src_ref=area(k, m), dst_ref=area(k, m), send_sem=ds.at[k, m],
             recv_sem=dr.at[k, m], device_id=partner, device_id_type=MESH,
         )
-
-    def l_copy(k):
-        return pltpu.make_async_copy(obuf.at[k, 0], area(k, 0, core), ls.at[k])
 
     for k in range(1, layers):
         z_copy(k).start()
     zbuf[0] = x_ref[...]
 
-    def forward(k):
+    def build(e):
+        wanted = lax.broadcasted_iota(jnp.int32, (cap, key_ref.shape[2]), 0)
+        sbuf[e] = jnp.where(key_ref[e] == wanted, 1.0, 0.0).astype(BF16)
+
+    def finish(k):
         @pl.loop(1, groups)
         def _(m):
             e_copy(k, m).wait_recv()
-            d_copy(k, m, area(k, m, core)).start()
+            d_copy(k, m).start()
+
+        @pl.loop(0, groups)
+        def _(m):
+            d_copy(k, m).wait_recv()
+
+        block = lax.rem(z + layers - k, layers)
+        depth = pl.ds(pl.multiple_of(block * 2 * cols, 128), 2 * cols)
+
+        @pl.loop(0, groups * cap // tile)
+        def _(t):
+            at = pl.ds(pl.multiple_of(t * tile, tile), tile)
+            left = jnp.concatenate([piece[0, k, at], piece[1, k, at]], axis=1)
+            gate = jnp.dot(left, wbuf[0, depth], preferred_element_type=jnp.float32)
+            up = jnp.dot(left, wbuf[1, depth], preferred_element_type=jnp.float32)
+
+            @pl.when(k == 0)
+            def _():
+                acc[0, at] = gate
+                acc[1, at] = up
+
+            @pl.when(jnp.logical_and(k > 0, k < layers - 1))
+            def _():
+                acc[0, at] += gate
+                acc[1, at] += up
+
+            @pl.when(k == layers - 1)
+            def _():
+                gates = acc[0, at] + gate
+                out_ref[at] = (gates / (1.0 + jnp.exp(-gates)) * (acc[1, at] + up)).astype(BF16)
 
     @pl.loop(0, layers)
     def _(k):
@@ -122,30 +155,41 @@
         @pl.loop(0, groups)
         def _(i):
             m = lax.rem(i + 1, groups)
-            obuf[k, m] = jnp.dot(
-                s_ref[lax.rem(g + m, groups)], zbuf[k], preferred_element_type=jnp.float32
-            ).astype(BF16)
+            e = lax.rem(g + m, groups)
+
+            @pl.when(k == 0)
+            def _():
+                build(e)
+
+            tile_out = jnp.dot(sbuf[e], zbuf[k], preferred_element_type=jnp.float32).astype(BF16)
 
             @pl.when(m > 0)
             def _():
+                obuf[k, m] = tile_out
                 e_copy(k, m).start()
 
-        l_copy(k).start()
-        d_copy(k, 0, obuf.at[k, 0]).start()
+            @pl.when(m == 0)
+            def _():
+                piece[core, k, pl.ds(pl.multiple_of(g * cap, 16), cap)] = tile_out
+
+        d_copy(k, 0).start()
+
+        @pl.when(k == 1)
+        def _():
+            for load in loads:
+                load.wait()
 
         @pl.when(k > 0)
         def _():
-            forward(k - 1)
-
-    forward(layers - 1)
+            finish(k - 1)
+
+    finish(layers - 1)
 
     @pl.loop(0, layers)
     def _(k):
         @pl.when(k > 0)
         def _():
             z_copy(k).wait_send()
-
-        l_copy(k).wait()
 
         @pl.loop(0, groups)
         def _(m):
@@ -153,54 +197,70 @@
             def _():
                 e_copy(k, m).wait_send()
 
-            copy = d_copy(k, m, obuf.at[k, 0])
-            copy.wait_send()
-            copy.wait_recv()
-
-
-def dispatch(normed, table):
-    groups, cap, tok_rows = table.shape
+            d_copy(k, m).wait_send()
+
+
+def tile_of(rows, cap):
+    return 384 if rows % 384 == 0 else cap
+
+
+def dispatch(normed, key, cap, gate_weight, up_weight):
+    tok_rows, groups = key.shape
     layers = lax.axis_size("tp") // 2
     cols = normed.shape[1]
+    rows = groups * cap
+    units = gate_weight.shape[1]
     vmem = pl.BlockSpec(memory_space=pltpu.VMEM)
+    hbm = pl.BlockSpec(memory_space=pl.ANY)
     return pl.pallas_call(
-        functools.partial(dispatch_kernel, groups, layers, cap, cols),
-        out_shape=jax.ShapeDtypeStruct((groups * cap, 2 * layers * cols), BF16),
-        in_specs=[vmem, vmem],
-        out_specs=pl.BlockSpec(memory_space=pl.ANY),
+        functools.partial(dispatch_kernel, groups, layers, cap, cols, tile_of(rows, cap)),
+        out_shape=jax.ShapeDtypeStruct((rows, units), BF16),
+        in_specs=[vmem, vmem, hbm, hbm],
+        out_specs=vmem,
         scratch_shapes=[
             pltpu.VMEM((layers, tok_rows, cols), BF16),
             pltpu.VMEM((layers, groups, cap, cols), BF16),
+            pltpu.VMEM((groups, cap, tok_rows), BF16),
+            pltpu.VMEM((2, layers, rows, cols), BF16),
+            pltpu.VMEM((2,) + gate_weight.shape, BF16),
+            pltpu.VMEM((2, rows, units), jnp.float32),
             DMA((layers,)), DMA((layers,)),
             DMA((layers, groups)), DMA((layers, groups)),
             DMA((layers, groups)), DMA((layers, groups)),
-            DMA((layers,)),
+            DMA((2,)),
         ],
         compiler_params=pltpu.CompilerParams(
-            collective_id=1, has_side_effects=True, vmem_limit_bytes=56 * 2**20
+            collective_id=1, has_side_effects=True, vmem_limit_bytes=60 * 2**20
         ),
         name="dispatch",
-    )(normed, table)
+    )(normed, key.T.reshape(groups, 1, tok_rows), gate_weight, up_weight)
 
 
 def return_kernel(
-    groups, layers, cap, cols, p_ref, w_ref, out_ref, lbuf, pbuf, qbuf, rbuf, obuf, fbuf,
-    ls, ds, dr, es, er, zs, zr,
+    groups, layers, cap, cols, tile, h_ref, down_ref, key_ref, weight_ref, out_ref,
+    wbuf, mix, lbuf, sbuf, pbuf, qbuf, rbuf, obuf, fbuf, ws, ds, dr, es, er, zs, zr,
 ):
     core, z, g, partner = places(groups, layers)
+    rows = groups * cap
+
+    def w_copy(k, other):
+        of = 1 - core if other else core
+        column = (lax.rem(z + k, layers) * 2 + of) * cols
+        return pltpu.make_async_copy(
+            down_ref.at[:, pl.ds(pl.multiple_of(column, 128), cols)], wbuf.at[k, other], ws.at[k, other]
+        )
+
+    @pl.loop(0, layers)
+    def _(i):
+        k = lax.rem(i + 1, layers)
+        w_copy(k, 1).start()
+        w_copy(k, 0).start()
+
     greet_all(groups, layers, core, z, g, partner)
-    rows = groups * cap
-
-    def columns(k, of):
-        column = (lax.rem(z + k, layers) * 2 + of) * cols
-        return p_ref.at[:, pl.ds(pl.multiple_of(column, 128), cols)]
-
-    def l_copy(k):
-        return pltpu.make_async_copy(columns(k, core), lbuf.at[k], ls.at[k])
 
     def d_copy(k):
         return pltpu.make_async_remote_copy(
-            src_ref=columns(k, 1 - core), dst_ref=pbuf.at[k], send_sem=ds.at[k],
+            src_ref=sbuf.at[k], dst_ref=pbuf.at[k], send_sem=ds.at[k],
             recv_sem=dr.at[k], device_id=partner, device_id_type=MESH,
         )
 
@@ -217,16 +277,22 @@
             device_id={"tp": lax.rem(z + k, layers) * 2 + core}, device_id_type=MESH,
         )
 
+    def project(k, other, target):
+        @pl.loop(0, rows // tile)
+        def _(t):
+            at = pl.ds(pl.multiple_of(t * tile, tile), tile)
+            target[k, at] = jnp.dot(
+                h_ref[at], wbuf[k, other], preferred_element_type=jnp.float32
+            ).astype(BF16)
+
     @pl.loop(0, layers)
     def _(i):
         k = lax.rem(i + 1, layers)
+        w_copy(k, 1).wait()
+        project(k, 1, sbuf)
         d_copy(k).start()
-        l_copy(k).start()
-
-    @pl.loop(0, layers)
-    def _(i):
-        k = lax.rem(i + 1, layers)
-        l_copy(k).wait()
+        w_copy(k, 0).wait()
+        project(k, 0, lbuf)
         d_copy(k).wait_recv()
 
         @pl.loop(0, groups)
@@ -244,8 +310,16 @@
             def _():
                 rbuf[k, pl.ds(pl.multiple_of(g * cap, 16), cap)] = both.astype(BF16)
 
-    tok_rows = w_ref.shape[0]
-    tile = min(256, tok_rows)
+        @pl.when(i == 0)
+        def _():
+            slots = lax.broadcasted_iota(jnp.int32, (mix.shape[1], cap), 1)
+            for e in range(groups):
+                mix[e] = jnp.where(
+                    key_ref[:, e : e + 1] == slots, weight_ref[:, e : e + 1], 0.0
+                ).astype(BF16)
+
+    tok_rows = mix.shape[1]
+    step = min(256, tok_rows)
 
     @pl.loop(0, layers)
     def _(i):
@@ -255,10 +329,14 @@
         def _(m):
             e_copy(k, m).wait_recv()
 
-        @pl.loop(0, tok_rows // tile)
+        @pl.loop(0, tok_rows // step)
         def _(t):
-            at = pl.ds(pl.multiple_of(t * tile, tile), tile)
-            value = jnp.dot(w_ref[at], rbuf[k], preferred_element_type=jnp.float32)
+            at = pl.ds(pl.multiple_of(t * step, step), step)
+            value = jnp.zeros((step, cols), jnp.float32)
+            for e in range(groups):
+                value += jnp.dot(
+                    mix[e, at], rbuf[k, e * cap : (e + 1) * cap], preferred_element_type=jnp.float32
+                )
 
             @pl.when(k > 0)
             def _():
@@ -290,34 +368,37 @@
             z_copy(k).wait_send()
 
 
-def give_back(partials, mixing, groups):
-    rows, width = partials.shape
-    tok_rows = mixing.shape[0]
+def give_back(hidden, down_weight, key, weight):
+    rows, units = hidden.shape
+    tok_rows, groups = key.shape
     layers = lax.axis_size("tp") // 2
-    cols = width // (2 * layers)
+    cols = down_weight.shape[1] // (2 * layers)
     cap = rows // groups
     vmem = pl.BlockSpec(memory_space=pltpu.VMEM)
+    hbm = pl.BlockSpec(memory_space=pl.ANY)
+    whole = pltpu.VMEM((layers, rows, cols), BF16)
     return pl.pallas_call(
-        functools.partial(return_kernel, groups, layers, cap, cols),
+        functools.partial(return_kernel, groups, layers, cap, cols, tile_of(rows, cap)),
         out_shape=jax.ShapeDtypeStruct((tok_rows, cols), jnp.float32),
-        in_specs=[pl.BlockSpec(memory_space=pl.ANY), vmem],
+        in_specs=[vmem, hbm, vmem, vmem],
         out_specs=vmem,
         scratch_shapes=[
-            pltpu.VMEM((layers, rows, cols), BF16),
-            pltpu.VMEM((layers, rows, cols), BF16),
+            pltpu.VMEM((layers, 2, units, cols), BF16),
+            pltpu.VMEM((groups, tok_rows, cap), BF16),
+            whole, whole, whole,
             pltpu.VMEM((layers, groups, cap, cols), BF16),
-            pltpu.VMEM((layers, rows, cols), BF16),
+            whole,
             pltpu.VMEM((layers, tok_rows, cols), BF16),
             pltpu.VMEM((layers, tok_rows, cols), BF16),
-            DMA((layers,)), DMA((layers,)), DMA((layers,)),
+            DMA((layers, 2)), DMA((layers,)), DMA((layers,)),
             DMA((layers, groups)), DMA((layers, groups)),
             DMA((layers,)), DMA((layers,)),
         ],
         compiler_params=pltpu.CompilerParams(
-            collective_id=2, has_side_effects=True, vmem_limit_bytes=56 * 2**20
+            collective_id=2, has_side_effects=True, vmem_limit_bytes=60 * 2**20
         ),
         name="give_back",
-    )(partials, mixing)
+    )(hidden, down_weight, key, weight)
 
 
 def on_device(
@@ -342,17 +423,9 @@
     before = (spot[:, None] > spot[None, :]).astype(BF16)
     rank = jnp.dot(before, member.astype(BF16), preferred_element_type=jnp.float32)
     key = jnp.where(member, rank.astype(jnp.int32), -1)
-    slots = jnp.arange(cap, dtype=jnp.int32)
-    table = (key.T[:, None, :] == slots[None, :, None]).astype(BF16)
-    mixing = jnp.where(key[:, :, None] == slots[None, None, :], weight[:, :, None], 0.0)
-    mixing = mixing.astype(BF16).reshape(tok_rows, groups * cap)
-
-    piece = dispatch(normed, table)
-    gate_act = jnp.dot(piece, gate_weight[0], preferred_element_type=jnp.float32)
-    up_act = jnp.dot(piece, up_weight[0], preferred_element_type=jnp.float32)
-    hidden = (jax.nn.silu(gate_act) * up_act).astype(BF16)
-    partials = jnp.dot(hidden, down_weight[0], preferred_element_type=jnp.float32).astype(BF16)
-    combined = give_back(partials, mixing, groups)
+
+    hidden = dispatch(normed, key, cap, gate_weight[0], up_weight[0])
+    combined = give_back(hidden, down_weight[0], key, weight)
     totals = sum_over_tp(jnp.sum(combined * combined, axis=1), 3)
     scaled = combined * lax.rsqrt(totals / width + epsilon)[:, None]
     return (scaled * post_gain.astype(jnp.float32)[None, :]).astype(BF16)

time: 263 us -> 198 us (0.75)
  matrix products: 41.8 us -> 0.69 us
  local copies, waits for them, and re-layouts: 24.2 us -> 2.12 us
  other arithmetic: 23.8 us -> 10.9 us
  Pallas kernels: 172 us -> 183 us
    dot_general x2 -> x0, matrix products: 41.4 us -> none  [the longest x1 26.9 us: on_device(): jnp.dot(hidden, down_weight[0], preferred_element_type=jnp.float32)]
    eq x4 -> x0, local copies, waits for them, and re-layouts: 14.7 us -> none  [on_device(): key[:, :, None] == slots[None, None, :]]
    convert_element_type x2 -> x0, other arithmetic: 12.5 us -> none  [the longest x1 8.44 us: on_device(): mixing = mixing.astype(BF16).reshape(tok_rows, groups * cap)]
    broadcast_in_dim x2 -> x0, local copies, waits for them, and re-layouts: 9.49 us -> none  [on_device(): jnp.where(key[:, :, None] == slots[None, None, :], weight[:, :, None], 0.0)]
    pallas_call x1, Pallas kernels: 71.5 us -> 77.9 us  [dispatch(): pl.pallas_call(functools.partial(dispatch_kernel, groups, layers, cap, co...]
    pallas_call x1, Pallas kernels: 85.4 us -> 89.3 us  [give_back(): pl.pallas_call(functools.partial(return_kernel, groups, layers, cap, cols...]
where the time goes in v2:
time: 198 us; the launch traced here: 197 us
  Pallas kernels  183 us (92%)
  other arithmetic  10.9 us (6%)
  local copies, waits for them, and re-layouts  2.12 us (1%)
    pallas_call x1, Pallas kernels, give_back(): pl.pallas_call(functools.partial(return_kernel, groups, layers, cap, cols...  89.3 us
    pallas_call x1, Pallas kernels, dispatch(): pl.pallas_call(functools.partial(dispatch_kernel, groups, layers, cap, co...  77.9 us
    pallas_call x2, Pallas kernels, sum_over_tp(): pl.pallas_call(functools.partial(exchange_kernel, n), out_shape=jax.Shape...  16.1 us

profile of v2, /device:TPU:0, one launch (start us, length us, event | category | flops | bytes accessed | tf_op | source)
XLA Modules:
  0.0 197.2 jit_solution(275489239109893834)
XLA Ops:
  0.0 0.7 fusion.6
  0.7 0.3 copy.14
  1.0 0.7 fusion.2.key_ref
  1.7 0.0 copy-start
  1.7 0.8 copy.15.key_ref
  2.5 1.8 fusion.3
  4.4 8.7 %exchange0.1 = f32[8,128]{1,0:T(8,128)} custom-call(f32[8,128]{1,0:T(8,128)} %bitcast.17), custom_call_target="tpu_custom_call" | custom-call | tf_op jit(solution)/shard_map/exchange0/pallas_call | solution.py:47
  13.1 0.7 rsqrt_bitcast_fusion.1
  13.7 0.7 convert_element_type.23
  14.4 2.0 %fusion.5.x_ref = bf16[1024,256]{1,0:T(8,128)(2,1)} fusion(bf16[1024,256]{1,0:T(8,128)(2,1)} %param.8, f32[256]{0:T(256)S(1)} %convert_element_type.23, f32[1024]{0:T(1024)S(1)} %rsqrt_bitcast_fusion.1), kind=kLoop, calls=%fused_computation.8 | loop fusion | flops 1048576 | bytes 1053696 | tf_op jit(solution)/shard_map/convert_element_type | solution.py:416
  16.4 0.0 copy-start.1
  16.5 0.0 copy-start.2
  16.5 77.9 %dispatch.1.h_ref = bf16[2304,896]{1,0:T(8,128)(2,1)} custom-call(bf16[1024,256]{1,0:T(8,128)(2,1)} %fusion.5.x_ref, s32[4,1,1024]{2,1,0:T(1,128)} %copy.15.key_ref, bf16[2048,896]{1,0:T(8,128)(2,1)} %bitcast.13, bf16[2048,896]{1,0:T(8,128)(2,1)} %bitcast.14), custom_call_target="tpu_custom_call" | custom-call | tf_op jit(solution)/shard_map/dispatch/pallas_call | solution.py:215
  94.4 0.0 copy-done
  94.4 0.0 copy-done.1
  94.4 0.0 copy-done.2
  94.5 1.0 copy.16.weight_ref
  95.5 0.0 copy-start.3
  95.5 89.3 %give_back.1 = f32[1024,256]{1,0:T(8,128)} custom-call(bf16[2304,896]{1,0:T(8,128)(2,1)} %dispatch.1.h_ref, bf16[896,2048]{1,0:T(8,128)(2,1)} %bitcast.15, s32[1024,4]{1,0:T(8,128)} %copy-done, f32[1024,4]{1,0:T(8,128)} %copy.16.weight_ref), custom_call_target="tpu_custom_call" | custom-call | tf_op jit(solution)/shard_map/give_back/pallas_call | solution.py:380
  184.8 2.0 %multiply_reduce_fusion = f32[1024]{0:T(1024)} fusion(f32[1024,256]{1,0:T(8,128)} %give_back.1), kind=kLoop, calls=%fused_computation.10 | loop fusion | flops 523264 | bytes 1052672 | tf_op jit(solution)/shard_map/reduce_sum | solution.py:429
  186.9 7.4 %exchange3.1 = f32[8,128]{1,0:T(8,128)} custom-call(f32[8,128]{1,0:T(8,128)} %bitcast.18), custom_call_target="tpu_custom_call" | custom-call | tf_op jit(solution)/shard_map/exchange3/pallas_call | solution.py:47
  194.3 0.7 rsqrt_bitcast_fusion
  195.0 0.0 copy-done.3
  195.0 2.2 %multiply_convert_fusion = bf16[1024,256]{1,0:T(8,128)(2,1)} fusion(f32[1024,256]{1,0:T(8,128)} %give_back.1, f32[256]{0:T(256)S(1)} %convert_element_type.26, f32[1024]{0:T(1024)S(1)} %rsqrt_bitcast_fusion), kind=kLoop, calls=%fused_computation.9 | loop fusion | flops 786432 | bytes 1577984 | tf_op jit(solution)/shard_map/convert_element_type | solution.py:431
  (2 shorter events, 0.0 us)
Async XLA Ops:
  1.7 92.7 %copy-start = (s32[1024,4]{1,0:T(8,128)}, s32[1024,4]{1,0:T(8,128)S(1)}, u32[]{:S(2)}) copy-start(s32[1024,4]{1,0:T(8,128)S(1)} %fusion.2.key_ref) | copy-start | bytes 49156
  16.4 78.0 %copy-start.1 = (s32[1024,2]{0,1:T(2,128)S(1)}, s32[1024,2]{0,1:T(2,128)}, u32[]{:S(2)}) copy-start(s32[1024,2]{0,1:T(2,128)} %param.10) | copy-start | bytes 24580
  16.5 78.0 %copy-start.2 = (f32[1024,2]{0,1:T(2,128)S(1)}, f32[1024,2]{0,1:T(2,128)}, u32[]{:S(2)}) copy-start(f32[1024,2]{0,1:T(2,128)} %param.11) | copy-start | bytes 24580
  95.5 99.5 %copy-start.3 = (bf16[256]{0:T(256)(128)(2,1)S(1)}, bf16[256]{0:T(256)(128)(2,1)}, u32[]{:S(2)}) copy-start(bf16[256]{0:T(256)(128)(2,1)} %param.15) | copy-start | bytes 1540

commit v3 on v2

--- a/solution.py
+++ b/solution.py
@@ -81,10 +81,27 @@
         load.start()
     greet_all(groups, layers, core, z, g, partner)
 
-    def z_copy(k):
-        return pltpu.make_async_remote_copy(
-            src_ref=x_ref, dst_ref=zbuf.at[k], send_sem=zs.at[k], recv_sem=zr.at[k],
-            device_id={"tp": lax.rem(z + k, layers) * 2 + core}, device_id_type=MESH,
+    def z_copy(source, to, at, sem):
+        return pltpu.make_async_remote_copy(
+            src_ref=source, dst_ref=zbuf.at[at], send_sem=zs.at[sem], recv_sem=zr.at[at],
+            device_id={"tp": to * 2 + core}, device_id_type=MESH,
+        )
+
+    def slot(s):
+        inner = jnp.minimum(z, layers - 1 - z)
+        near = jnp.where(s % 2 == 1, (s + 1) // 2, layers - (s + 1) // 2)
+        far = jnp.where(2 * z > layers - 1, s - inner, layers - s + inner)
+        return jnp.where(s == 0, 0, jnp.where(s <= 2 * inner, near, far))
+
+    to_right = z_copy(x_ref, z + 1, 1, 0)
+    to_left = z_copy(x_ref, z - 1, layers - 1, layers)
+
+    def relays(k):
+        right = jnp.logical_and(jnp.logical_and(k > 0, z >= k), z < layers - 1)
+        left = jnp.logical_and(z < k, z > 0)
+        return (
+            (right, z_copy(zbuf.at[k], z + 1, k + 1, k)),
+            (left, z_copy(zbuf.at[k], z - 1, k - 1, k)),
         )
 
     def area(k, m):
@@ -103,15 +120,17 @@
             recv_sem=dr.at[k, m], device_id=partner, device_id_type=MESH,
         )
 
-    for k in range(1, layers):
-        z_copy(k).start()
+    pl.when(z < layers - 1)(to_right.start)
+    pl.when(z > 0)(to_left.start)
     zbuf[0] = x_ref[...]
 
     def build(e):
         wanted = lax.broadcasted_iota(jnp.int32, (cap, key_ref.shape[2]), 0)
         sbuf[e] = jnp.where(key_ref[e] == wanted, 1.0, 0.0).astype(BF16)
 
-    def finish(k):
+    def finish(s):
+        k = slot(s)
+
         @pl.loop(1, groups)
         def _(m):
             e_copy(k, m).wait_recv()
@@ -131,33 +150,37 @@
             gate = jnp.dot(left, wbuf[0, depth], preferred_element_type=jnp.float32)
             up = jnp.dot(left, wbuf[1, depth], preferred_element_type=jnp.float32)
 
-            @pl.when(k == 0)
+            @pl.when(s == 0)
             def _():
                 acc[0, at] = gate
                 acc[1, at] = up
 
-            @pl.when(jnp.logical_and(k > 0, k < layers - 1))
+            @pl.when(jnp.logical_and(s > 0, s < layers - 1))
             def _():
                 acc[0, at] += gate
                 acc[1, at] += up
 
-            @pl.when(k == layers - 1)
+            @pl.when(s == layers - 1)
             def _():
                 gates = acc[0, at] + gate
                 out_ref[at] = (gates / (1.0 + jnp.exp(-gates)) * (acc[1, at] + up)).astype(BF16)
 
     @pl.loop(0, layers)
-    def _(k):
-        @pl.when(k > 0)
-        def _():
-            z_copy(k).wait_recv()
+    def _(s):
+        k = slot(s)
+
+        @pl.when(s > 0)
+        def _():
+            z_copy(x_ref, lax.rem(z + 1, layers), k, k).wait_recv()
+            for wanted, copy in relays(k):
+                pl.when(wanted)(copy.start)
 
         @pl.loop(0, groups)
         def _(i):
             m = lax.rem(i + 1, groups)
             e = lax.rem(g + m, groups)
 
-            @pl.when(k == 0)
+            @pl.when(s == 0)
             def _():
                 build(e)
 
@@ -174,22 +197,23 @@
 
         d_copy(k, 0).start()
 
-        @pl.when(k == 1)
+        @pl.when(s == 1)
         def _():
             for load in loads:
                 load.wait()
 
-        @pl.when(k > 0)
-        def _():
-            finish(k - 1)
+        @pl.when(s > 0)
+        def _():
+            finish(s - 1)
 
     finish(layers - 1)
+    pl.when(z < layers - 1)(to_right.wait_send)
+    pl.when(z > 0)(to_left.wait_send)
 
     @pl.loop(0, layers)
     def _(k):
-        @pl.when(k > 0)
-        def _():
-            z_copy(k).wait_send()
+        for wanted, copy in relays(k):
+            pl.when(wanted)(copy.wait_send)
 
         @pl.loop(0, groups)
         def _(m):
@@ -224,7 +248,7 @@
             pltpu.VMEM((2, layers, rows, cols), BF16),
             pltpu.VMEM((2,) + gate_weight.shape, BF16),
             pltpu.VMEM((2, rows, units), jnp.float32),
-            DMA((layers,)), DMA((layers,)),
+            DMA((layers + 1,)), DMA((layers,)),
             DMA((layers, groups)), DMA((layers, groups)),
             DMA((layers, groups)), DMA((layers, groups)),
             DMA((2,)),

time: 198 us -> 191 us (0.965)
  Pallas kernels: 183 us -> 176 us
    pallas_call x1, Pallas kernels: 89.3 us -> 76.9 us  [give_back(): pl.pallas_call(functools.partial(return_kernel, groups, layers, cap, cols...]
    pallas_call x1, Pallas kernels: 77.9 us -> 81.4 us  [dispatch(): pl.pallas_call(functools.partial(dispatch_kernel, groups, layers, cap, co...]
where the time goes in v3:
time: 191 us; the launch traced here: 190 us
  Pallas kernels  176 us (92%)
  other arithmetic  10.9 us (6%)
  local copies, waits for them, and re-layouts  2.12 us (1%)
    pallas_call x1, Pallas kernels, dispatch(): pl.pallas_call(functools.partial(dispatch_kernel, groups, layers, cap, co...  81.4 us
    pallas_call x1, Pallas kernels, give_back(): pl.pallas_call(functools.partial(return_kernel, groups, layers, cap, cols...  76.9 us
    pallas_call x2, Pallas kernels, sum_over_tp(): pl.pallas_call(functools.partial(exchange_kernel, n), out_shape=jax.Shape...  18 us

profile of v3, /device:TPU:0, one launch (start us, length us, event | category | flops | bytes accessed | tf_op | source)
XLA Modules:
  0.0 190.1 jit_solution(12789815820155615545)
XLA Ops:
  0.0 0.7 fusion.6
  0.7 0.3 copy.14
  1.0 0.7 fusion.2.key_ref
  1.7 0.0 copy-start
  1.7 0.8 copy.15.key_ref
  2.5 1.8 fusion.3
  4.4 8.7 %exchange0.1 = f32[8,128]{1,0:T(8,128)} custom-call(f32[8,128]{1,0:T(8,128)} %bitcast.17), custom_call_target="tpu_custom_call" | custom-call | tf_op jit(solution)/shard_map/exchange0/pallas_call | solution.py:47
  13.1 0.7 rsqrt_bitcast_fusion.1
  13.7 0.7 convert_element_type.23
  14.4 2.0 %fusion.5.x_ref = bf16[1024,256]{1,0:T(8,128)(2,1)} fusion(bf16[1024,256]{1,0:T(8,128)(2,1)} %param.8, f32[256]{0:T(256)S(1)} %convert_element_type.23, f32[1024]{0:T(1024)S(1)} %rsqrt_bitcast_fusion.1), kind=kLoop, calls=%fused_computation.8 | loop fusion | flops 1048576 | bytes 1053696 | tf_op jit(solution)/shard_map/convert_element_type | solution.py:440
  16.4 0.0 copy-start.1
  16.5 0.0 copy-start.2
  16.5 81.4 %dispatch.1.h_ref = bf16[2304,896]{1,0:T(8,128)(2,1)} custom-call(bf16[1024,256]{1,0:T(8,128)(2,1)} %fusion.5.x_ref, s32[4,1,1024]{2,1,0:T(1,128)} %copy.15.key_ref, bf16[2048,896]{1,0:T(8,128)(2,1)} %bitcast.13, bf16[2048,896]{1,0:T(8,128)(2,1)} %bitcast.14), custom_call_target="tpu_custom_call" | custom-call | tf_op jit(solution)/shard_map/dispatch/pallas_call | solution.py:239
  97.9 0.0 copy-done
  97.9 0.0 copy-done.1
  97.9 0.0 copy-done.2
  97.9 1.0 copy.16.weight_ref
  98.9 0.0 copy-start.3
  98.9 76.9 %give_back.1 = f32[1024,256]{1,0:T(8,128)} custom-call(bf16[2304,896]{1,0:T(8,128)(2,1)} %dispatch.1.h_ref, bf16[896,2048]{1,0:T(8,128)(2,1)} %bitcast.15, s32[1024,4]{1,0:T(8,128)} %copy-done, f32[1024,4]{1,0:T(8,128)} %copy.16.weight_ref), custom_call_target="tpu_custom_call" | custom-call | tf_op jit(solution)/shard_map/give_back/pallas_call | solution.py:404
  175.9 2.0 %multiply_reduce_fusion = f32[1024]{0:T(1024)} fusion(f32[1024,256]{1,0:T(8,128)} %give_back.1), kind=kLoop, calls=%fused_computation.10 | loop fusion | flops 523264 | bytes 1052672 | tf_op jit(solution)/shard_map/reduce_sum | solution.py:453
  177.9 9.3 %exchange3.1 = f32[8,128]{1,0:T(8,128)} custom-call(f32[8,128]{1,0:T(8,128)} %bitcast.18), custom_call_target="tpu_custom_call" | custom-call | tf_op jit(solution)/shard_map/exchange3/pallas_call | solution.py:47
  187.2 0.7 rsqrt_bitcast_fusion
  187.9 0.0 copy-done.3
  187.9 2.2 %multiply_convert_fusion = bf16[1024,256]{1,0:T(8,128)(2,1)} fusion(f32[1024,256]{1,0:T(8,128)} %give_back.1, f32[256]{0:T(256)S(1)} %convert_element_type.26, f32[1024]{0:T(1024)S(1)} %rsqrt_bitcast_fusion), kind=kLoop, calls=%fused_computation.9 | loop fusion | flops 786432 | bytes 1577984 | tf_op jit(solution)/shard_map/convert_element_type | solution.py:455
  (2 shorter events, 0.0 us)
Async XLA Ops:
  1.7 96.2 %copy-start = (s32[1024,4]{1,0:T(8,128)}, s32[1024,4]{1,0:T(8,128)S(1)}, u32[]{:S(2)}) copy-start(s32[1024,4]{1,0:T(8,128)S(1)} %fusion.2.key_ref) | copy-start | bytes 49156
  16.4 81.4 %copy-start.1 = (s32[1024,2]{0,1:T(2,128)S(1)}, s32[1024,2]{0,1:T(2,128)}, u32[]{:S(2)}) copy-start(s32[1024,2]{0,1:T(2,128)} %param.10) | copy-start | bytes 24580
  16.5 81.4 %copy-start.2 = (f32[1024,2]{0,1:T(2,128)S(1)}, f32[1024,2]{0,1:T(2,128)}, u32[]{:S(2)}) copy-start(f32[1024,2]{0,1:T(2,128)} %param.11) | copy-start | bytes 24580
  98.9 88.9 %copy-start.3 = (bf16[256]{0:T(256)(128)(2,1)S(1)}, bf16[256]{0:T(256)(128)(2,1)}, u32[]{:S(2)}) copy-start(bf16[256]{0:T(256)(128)(2,1)} %param.15) | copy-start | bytes 1540
